TPU v7x, 32 devices: a whole 2x2x4 slice. The times are simulated.
32 devices in a mesh: rep: 2 (over x), fs: 8 (over z, y), tp: 2 (over core).
Axes of the slice: x: 2, y: 2, z: 4, core: 2. Of those that a mesh axis runs over, the one named last changes fastest.
Arguments:
- resid: bfloat16 [4096, 2048], P(('rep', 'fs'), 'tp'), may hold values from -6 to 6
- norm_gains: float32 [3, 2048], replicated, may hold values from 0.1 to 1.9
- gate_one: bfloat16 [2048, 5632], P('fs', 'tp'), may hold values from -0.125 to 0.125
- up_one: bfloat16 [2048, 5632], P('fs', 'tp'), may hold values from -0.125 to 0.125
- down_one: bfloat16 [5632, 2048], P('tp', 'fs'), may hold values from -0.109375 to 0.109375
- proj_u: bfloat16 [2048, 1024], P('fs', 'tp'), may hold values from -0.125 to 0.125
- proj_v: bfloat16 [2048, 1024], P('fs', 'tp'), may hold values from -0.125 to 0.125
- spatial: bfloat16 [8, 128, 128], P('tp'), may hold values from -0.5 to 0.5
- spatial_bias: float32 [8, 128], P('tp'), may hold values from 0.1 to 1.9
- mix_gain: float32 [1024], P('tp'), may hold values from 0.1 to 1.9
- head_gain: float32 [1024], P('tp'), may hold values from 0.1 to 1.9
- proj_out: bfloat16 [1024, 2048], P('tp', 'fs'), may hold values from -0.25 to 0.25
- gate_two: bfloat16 [2048, 5632], P('fs', 'tp'), may hold values from -0.125 to 0.125
- up_two: bfloat16 [2048, 5632], P('fs', 'tp'), may hold values from -0.125 to 0.125
- down_two: bfloat16 [5632, 2048], P('tp', 'fs'), may hold values from -0.109375 to 0.109375
Outputs:
- layer_out: bfloat16 [4096, 2048], P(('rep', 'fs'), 'tp')
All inputs are finite; a program needn't handle non-finite values.
Results may differ from a plain program's by a relative error of at most 0.019.
Values may be sent and summed in bfloat16 or wider, within the bound.
A program may use at most 128 MiB of HBM per device.

v0:
```python
import jax
import jax.numpy as jnp
from jax import lax
from jax.sharding import PartitionSpec as P

HEAD_DIM = 128
BLOCK = 128
SPAN = 64


def rms_scale(values, gain):
    return values * lax.rsqrt(jnp.mean(values * values, axis=-1, keepdims=True) + 1e-06) * gain


def normalized(stream, gain):
    whole = lax.all_gather(stream, "tp", axis=1, tiled=True).astype(jnp.float32)
    return rms_scale(whole, gain).astype(jnp.bfloat16)


def accumulate(left, piece):
    return jnp.dot(left, piece, preferred_element_type=jnp.float32)


def folders(normed):

    def single(total, piece, start):
        return accumulate(normed, piece)

    def double(totals, pieces, start):
        return (accumulate(normed, pieces[0]), accumulate(normed, pieces[1]))

    return (single, double)


def ffn_inputs(normed, first_weight, second_weight):
    empty = jnp.zeros((normed.shape[0], first_weight.shape[1]), jnp.float32)
    single, double = folders(normed)
    result = (
        single(empty, lax.all_gather(first_weight, "fs", axis=0, tiled=True), jnp.int32(0)),
        single(empty, lax.all_gather(second_weight, "fs", axis=0, tiled=True), jnp.int32(0)),
    )
    return result


def mixer_inputs(normed, first_weight, second_weight):
    empty = jnp.zeros((normed.shape[0], first_weight.shape[1]), jnp.float32)
    single, double = folders(normed)
    result = (
        single(empty, lax.all_gather(first_weight, "fs", axis=0, tiled=True), jnp.int32(0)),
        single(empty, lax.all_gather(second_weight, "fs", axis=0, tiled=True), jnp.int32(0)),
    )
    return result


def feed_forward(stream, gain, gate_weight, up_weight, down_weight):
    normed = normalized(stream, gain)
    gate, up_part = ffn_inputs(normed, gate_weight, up_weight)
    hidden = (jax.nn.silu(gate) * up_part).astype(jnp.bfloat16)
    terms = jnp.dot(
        hidden,
        lax.all_gather(down_weight, "fs", axis=1, tiled=True),
        preferred_element_type=jnp.float32,
    )
    return lax.psum_scatter(
        terms.astype(jnp.bfloat16), "tp", scatter_dimension=1, tiled=True
    ).astype(jnp.float32)


def body(
    resid,
    norm_gains,
    gate_one,
    up_one,
    down_one,
    proj_u,
    proj_v,
    spatial,
    spatial_bias,
    mix_gain,
    head_gain,
    proj_out,
    gate_two,
    up_two,
    down_two,
):
    first = (
        resid.astype(jnp.float32)
        + 0.5 * feed_forward(resid, norm_gains[0], gate_one, up_one, down_one)
    ).astype(jnp.bfloat16)
    mnormed = normalized(first, norm_gains[1])
    u_part, v_part = mixer_inputs(mnormed, proj_u, proj_v)
    rows = u_part.shape[0]
    seqs = rows // BLOCK
    local_heads = spatial.shape[0]
    gated_u = jax.nn.gelu(u_part).reshape(seqs, BLOCK, local_heads, HEAD_DIM)
    gated_v = jax.nn.gelu(v_part).reshape(seqs, BLOCK, local_heads, HEAD_DIM)
    centre = jnp.mean(gated_v, axis=-1, keepdims=True)
    spread = jnp.mean(jnp.square(gated_v - centre), axis=-1, keepdims=True)
    vn = (
        (gated_v - centre) * lax.rsqrt(spread + 1e-05) * mix_gain.reshape(local_heads, HEAD_DIM)
    ).astype(jnp.bfloat16)
    segment = jnp.arange(BLOCK) // SPAN
    causal = segment[:, None] >= segment[None, :]
    masked = jnp.where(causal[None], spatial, jnp.zeros_like(spatial))
    mixed = (
        jnp.einsum("hts,bshd->bthd", masked, vn, preferred_element_type=jnp.float32)
        + spatial_bias.T[None, :, :, None]
    )
    product = gated_u * mixed
    gated = (
        rms_scale(product, head_gain.reshape(local_heads, HEAD_DIM))
        .astype(jnp.bfloat16)
        .reshape(rows, local_heads * HEAD_DIM)
    )
    terms = jnp.dot(
        gated,
        lax.all_gather(proj_out, "fs", axis=1, tiled=True),
        preferred_element_type=jnp.float32,
    )
    branch = lax.psum_scatter(
        terms.astype(jnp.bfloat16), "tp", scatter_dimension=1, tiled=True
    ).astype(jnp.float32)
    second = (first.astype(jnp.float32) + branch).astype(jnp.bfloat16)
    return (
        second.astype(jnp.float32)
        + 0.5 * feed_forward(second, norm_gains[2], gate_two, up_two, down_two)
    ).astype(jnp.bfloat16)


def solution(mesh):
    return jax.shard_map(
        body,
        mesh=mesh,
        in_specs=(
            P(("rep", "fs"), "tp"),
            P(),
            P("fs", "tp"),
            P("fs", "tp"),
            P("tp", "fs"),
            P("fs", "tp"),
            P("fs", "tp"),
            P("tp", None, None),
            P("tp", None),
            P("tp"),
            P("tp"),
            P("tp", "fs"),
            P("fs", "tp"),
            P("fs", "tp"),
            P("tp", "fs"),
        ),
        out_specs=P(("rep", "fs"), "tp"),
        check_vma=False,
    )
```

profile of v0, /device:TPU:0, one launch (start us, length us, event | category | flops | bytes accessed | tf_op | source)
XLA Modules:
  0.0 1249.6 jit_solution(18036536609413237161)
XLA Ops:
  6.5 0.7 all-gather.13.cloned.1.call-update
  7.3 0.7 all-gather.15.cloned.1.call-update
  9.4 11.2 all-gather.13.cloned.1.call-done
  20.7 1.5 fusion.2
  22.2 165.2 %all-gather.15.cloned.1.call-done = bf16[2048,2816]{1,0:T(8,128)(2,1)} async-done(((bf16[256,2816]{1,0:T(8,128)(2,1)}), bf16[2048,2816]{1,0:T(8,128)(2,1)}) %all-gather.15.cloned.1.call-update) | async-done | bytes 11534352 | tf_op jit(solution)/shard_map/all_gather | solution.py:39
  187.4 9.5 fusion.41
  196.9 154.2 %all-gather.17.cloned.1.call-done = bf16[2048,2816]{1,0:T(8,128)(2,1)} async-done(((bf16[256,2816]{1,0:T(8,128)(2,1)}), bf16[2048,2816]{1,0:T(8,128)(2,1)}) %all-gather.17.cloned.1.call-update) | async-done | bytes 11534352 | tf_op jit(solution)/shard_map/all_gather | solution.py:40
  351.1 163.4 %all-gather.19.cloned.1.call-done = bf16[2816,2048]{1,0:T(8,128)(2,1)} async-done(((bf16[2816,256]{1,0:T(8,128)(2,1)}), bf16[2816,2048]{1,0:T(8,128)(2,1)}) %all-gather.19.cloned.1.call-update) | async-done | bytes 11534352 | tf_op jit(solution)/shard_map/all_gather | solution.py:61
  514.5 15.6 %convolution_convert_fusion.2 = bf16[256,2048]{1,0:T(8,128)(2,1)} fusion(bf16[2816,2048]{1,0:T(8,128)(2,1)} %all-gather.19.cloned.1.call-done, bf16[2048,2816]{1,0:T(8,128)(2,1)} %all-gather.17.cloned.1.call-done, f32[256,2816]{1,0:T(8,128)} %fusion.41, bf16[256,2048]{1,0:T(8,128)(2,1)S(1)} %copy-done.3, f32[2048]{0:T(1024)S(1)} %bitcast.39, ...), kind=kOutput, calls=%fused_computation.12 | convolution fusion | flops 5912526848 | bytes 28058624 | tf_op jit(solution)/shard_map/dot_general | solution.py:59
  530.2 6.7 reduce-scatter.4.cloned.1.call-done
  536.9 2.0 add_convert_fusion.2
  539.0 0.7 all-gather.25.cloned.1.call-update
  541.5 7.8 all-gather.21.cloned.1.call-done
  549.3 1.5 fusion.5
  550.8 50.9 %all-gather.25.cloned.1.call-done = bf16[2048,512]{1,0:T(8,128)(2,1)} async-done(((bf16[256,512]{1,0:T(8,128)(2,1)}), bf16[2048,512]{1,0:T(8,128)(2,1)}) %all-gather.25.cloned.1.call-update) | async-done | bytes 2097168 | tf_op jit(solution)/shard_map/all_gather | solution.py:50
  601.7 2.8 fusion.26
  604.7 46.7 %all-gather.23.cloned.1.call-done = bf16[2048,512]{1,0:T(8,128)(2,1)} async-done(((bf16[256,512]{1,0:T(8,128)(2,1)}), bf16[2048,512]{1,0:T(8,128)(2,1)}) %all-gather.23.cloned.1.call-update) | async-done | bytes 2097168 | tf_op jit(solution)/shard_map/all_gather | solution.py:49
  651.5 2.4 fusion.19
  656.7 45.7 %all-gather.27.cloned.1.call-done = bf16[512,2048]{1,0:T(8,128)(2,1)} async-done(((bf16[512,256]{1,0:T(8,128)(2,1)}), bf16[512,2048]{1,0:T(8,128)(2,1)}) %all-gather.27.cloned.1.call-update) | async-done | bytes 2097168 | tf_op jit(solution)/shard_map/all_gather | solution.py:117
  702.4 3.4 convolution_convert_fusion.1
  705.9 6.7 reduce-scatter.6.cloned.1.call-done
  712.5 2.0 add_convert_fusion.1
  715.2 0.7 all-gather.33.cloned.1.call-update
  716.8 8.2 all-gather.29.cloned.1.call-done
  724.9 1.5 fusion.8
  726.5 165.0 %all-gather.31.cloned.1.call-done = bf16[2048,2816]{1,0:T(8,128)(2,1)} async-done(((bf16[256,2816]{1,0:T(8,128)(2,1)}), bf16[2048,2816]{1,0:T(8,128)(2,1)}) %all-gather.31.cloned.1.call-update) | async-done | bytes 11534352 | tf_op jit(solution)/shard_map/all_gather | solution.py:39
  891.5 9.5 fusion.29
  901.0 154.2 %all-gather.33.cloned.1.call-done = bf16[2048,2816]{1,0:T(8,128)(2,1)} async-done(((bf16[256,2816]{1,0:T(8,128)(2,1)}), bf16[2048,2816]{1,0:T(8,128)(2,1)}) %all-gather.33.cloned.1.call-update) | async-done | bytes 11534352 | tf_op jit(solution)/shard_map/all_gather | solution.py:40
  1055.2 163.4 %all-gather.35.cloned.1.call-done = bf16[2816,2048]{1,0:T(8,128)(2,1)} async-done(((bf16[2816,256]{1,0:T(8,128)(2,1)}), bf16[2816,2048]{1,0:T(8,128)(2,1)}) %all-gather.35.cloned.1.call-update) | async-done | bytes 11534352 | tf_op jit(solution)/shard_map/all_gather | solution.py:61
  1218.6 15.6 %convolution_convert_fusion = bf16[256,2048]{1,0:T(8,128)(2,1)} fusion(bf16[2816,2048]{1,0:T(8,128)(2,1)} %all-gather.35.cloned.1.call-done, bf16[2048,2816]{1,0:T(8,128)(2,1)} %all-gather.33.cloned.1.call-done, f32[256,2816]{1,0:T(8,128)} %fusion.29, bf16[256,2048]{1,0:T(8,128)(2,1)S(1)} %copy-done.5, f32[2048]{0:T(1024)S(1)} %bitcast.35, ...), kind=kOutput, calls=%fused_computation.10 | convolution fusion | flops 5912526848 | bytes 28058624 | tf_op jit(solution)/shard_map/dot_general | solution.py:59
  1234.3 6.7 reduce-scatter.8.cloned.1.call-done
  1241.0 2.0 add_convert_fusion
  (67 shorter events, 7.7 us)
Async XLA Ops:
  6.5 14.1 %all-gather.13.cloned.1.call-start = ((), (), s32[]{:S(2)}) async-start(), calls=%async_computation.3 | async-start | bytes 1572864 | tf_op jit(solution)/shard_map/all_gather | solution.py:16
  7.3 2.1 copy-start.7
  7.3 180.1 %all-gather.15.cloned.1.call-start = ((), (), s32[]{:S(2)}) async-start(), calls=%async_computation.4 | async-start | bytes 12976128 | tf_op jit(solution)/shard_map/all_gather | solution.py:39
  8.0 343.1 %all-gather.17.cloned.1.call-start = ((), (), s32[]{:S(2)}) async-start(), calls=%async_computation.5 | async-start | bytes 12976128 | tf_op jit(solution)/shard_map/all_gather | solution.py:40
  8.8 505.8 %all-gather.19.cloned.1.call-start = ((), (), s32[]{:S(2)}) async-start(), calls=%async_computation.6 | async-start | bytes 12976128 | tf_op jit(solution)/shard_map/all_gather | solution.py:61
  9.3 527.6 %reduce-scatter.4.cloned.1.call-start = ((), (), s32[]{:S(2)}) async-start(), calls=%async_computation.7 | async-start | bytes 1572864 | tf_op jit(solution)/shard_map/reduce_scatter | solution.py:64
  187.4 327.2 %copy-start.3 = (bf16[256,2048]{1,0:T(8,128)(2,1)S(1)}, bf16[256,2048]{1,0:T(8,128)(2,1)}, u32[]{:S(2)}) copy-start(bf16[256,2048]{1,0:T(8,128)(2,1)} %all-gather.13.cloned.1.call-done) | copy-start | bytes 3145732
  196.9 340.0 %copy-start.2 = (bf16[256,1024]{1,0:T(8,128)(2,1)S(1)}, bf16[256,1024]{1,0:T(8,128)(2,1)}, u32[]{:S(2)}) copy-start(bf16[256,1024]{1,0:T(8,128)(2,1)} %param.15) | copy-start | bytes 1572868
  530.1 19.1 %all-gather.21.cloned.1.call-start = ((), (), s32[]{:S(2)}) async-start(), calls=%async_computation.8 | async-start | bytes 1572864 | tf_op jit(solution)/shard_map/all_gather | solution.py:16
  538.9 62.8 %all-gather.25.cloned.1.call-start = ((), (), s32[]{:S(2)}) async-start(), calls=%async_computation.10 | async-start | bytes 2359296 | tf_op jit(solution)/shard_map/all_gather | solution.py:50
  539.7 111.8 %all-gather.23.cloned.1.call-start = ((), (), s32[]{:S(2)}) async-start(), calls=%async_computation.9 | async-start | bytes 2359296 | tf_op jit(solution)/shard_map/all_gather | solution.py:49
  540.4 162.0 %all-gather.27.cloned.1.call-start = ((), (), s32[]{:S(2)}) async-start(), calls=%async_computation.11 | async-start | bytes 2359296 | tf_op jit(solution)/shard_map/all_gather | solution.py:117
  541.2 171.4 %reduce-scatter.6.cloned.1.call-start = ((), (), s32[]{:S(2)}) async-start(), calls=%async_computation.12 | async-start | bytes 1572864 | tf_op jit(solution)/shard_map/reduce_scatter | solution.py:120
  601.7 49.8 %copy-start.4 = (bf16[256,2048]{1,0:T(8,128)(2,1)S(1)}, bf16[256,2048]{1,0:T(8,128)(2,1)}, u32[]{:S(2)}) copy-start(bf16[256,2048]{1,0:T(8,128)(2,1)} %all-gather.21.cloned.1.call-done) | copy-start | bytes 3145732
  653.9 1.5 copy-start.8
  654.1 1.9 copy-start.6
  654.1 1.9 copy-start.9
  654.4 2.0 copy-start.10
  702.4 10.1 copy-start
  705.8 19.1 %all-gather.29.cloned.1.call-start = ((), (), s32[]{:S(2)}) async-start(), calls=%async_computation.13 | async-start | bytes 1572864 | tf_op jit(solution)/shard_map/all_gather | solution.py:16
  714.6 176.9 %all-gather.31.cloned.1.call-start = ((), (), s32[]{:S(2)}) async-start(), calls=%async_computation.14 | async-start | bytes 12976128 | tf_op jit(solution)/shard_map/all_gather | solution.py:39
  715.2 340.0 %all-gather.33.cloned.1.call-start = ((), (), s32[]{:S(2)}) async-start(), calls=%async_computation.15 | async-start | bytes 12976128 | tf_op jit(solution)/shard_map/all_gather | solution.py:40
  715.9 502.7 %all-gather.35.cloned.1.call-start = ((), (), s32[]{:S(2)}) async-start(), calls=%async_computation.16 | async-start | bytes 12976128 | tf_op jit(solution)/shard_map/all_gather | solution.py:61
  716.5 524.5 %reduce-scatter.8.cloned.1.call-start = ((), (), s32[]{:S(2)}) async-start(), calls=%async_computation.17 | async-start | bytes 1572864 | tf_op jit(solution)/shard_map/reduce_scatter | solution.py:64
  891.5 327.1 %copy-start.5 = (bf16[256,2048]{1,0:T(8,128)(2,1)S(1)}, bf16[256,2048]{1,0:T(8,128)(2,1)}, u32[]{:S(2)}) copy-start(bf16[256,2048]{1,0:T(8,128)(2,1)} %all-gather.29.cloned.1.call-done) | copy-start | bytes 3145732
  901.0 340.0 %copy-start.1 = (bf16[256,1024]{1,0:T(8,128)(2,1)S(1)}, bf16[256,1024]{1,0:T(8,128)(2,1)}, u32[]{:S(2)}) copy-start(bf16[256,1024]{1,0:T(8,128)(2,1)} %add_convert_fusion.1) | copy-start | bytes 1572868
Sparse Core Ops, SparseCore 0:
  8.9 11.7 all-gather.12
  22.8 164.4 all-gather.14
  189.6 161.4 all-gather.16
  353.0 161.4 all-gather.18
  530.3 6.5 reduce-scatter.3
  539.1 10.1 all-gather.20
  551.4 50.2 all-gather.24
  603.8 47.6 all-gather.22
  653.5 48.8 all-gather.26
  705.9 6.5 reduce-scatter.5
  714.7 10.1 all-gather.28
  727.0 164.4 all-gather.30
  893.7 161.4 all-gather.32
  1057.1 161.4 all-gather.34
  1234.4 6.5 reduce-scatter.7
where the time goes:
time: 1250 us
  waiting for transfers between devices  1160 us (93%)
  matrix products  59.1 us (5%)
  between operations  13.5 us (1%)
  other arithmetic  12.5 us (1%)
    all_gather x2, waiting for transfers between devices, ffn_inputs(): lax.all_gather(first_weight, 'fs', axis=0, tiled=True)  330 us
    all_gather x2, waiting for transfers between devices, feed_forward(): lax.all_gather(down_weight, 'fs', axis=1, tiled=True)  327 us
    all_gather x2, waiting for transfers between devices, ffn_inputs(): lax.all_gather(second_weight, 'fs', axis=0, tiled=True)  308 us
    all_gather x1, waiting for transfers between devices, mixer_inputs(): lax.all_gather(second_weight, 'fs', axis=0, tiled=True)  50.9 us
    all_gather x1, waiting for transfers between devices, mixer_inputs(): lax.all_gather(first_weight, 'fs', axis=0, tiled=True)  46.7 us
    all_gather x1, waiting for transfers between devices, body(): lax.all_gather(proj_out, 'fs', axis=1, tiled=True)  45.7 us
    dot_general x2, matrix products, feed_forward(): jnp.dot(hidden, lax.all_gather(down_weight, 'fs', axis=1, tiled=True), pr...  31.2 us
    all_gather x3, waiting for transfers between devices, normalized(): whole = lax.all_gather(stream, 'tp', axis=1, tiled=True).astype(jnp.float32)  27.2 us
  transfers between devices with their start and end apart: 15, of which 15 were waited for; matrix products, arithmetic and copies ran while one was open for 3% of the time, Pallas kernels for 0%

commit v1 on v0

--- a/solution.py
+++ b/solution.py
@@ -1,7 +1,12 @@
+import functools
+
 import jax
 import jax.numpy as jnp
 from jax import lax
+from jax.experimental import pallas as pl
+from jax.experimental.pallas import tpu as pltpu
 from jax.sharding import PartitionSpec as P
+
 
 HEAD_DIM = 128
 BLOCK = 128
@@ -34,7 +39,7 @@
 
 def ffn_inputs(normed, first_weight, second_weight):
     empty = jnp.zeros((normed.shape[0], first_weight.shape[1]), jnp.float32)
-    single, double = folders(normed)
+    single, _ = folders(normed)
     result = (
         single(empty, lax.all_gather(first_weight, "fs", axis=0, tiled=True), jnp.int32(0)),
         single(empty, lax.all_gather(second_weight, "fs", axis=0, tiled=True), jnp.int32(0)),
@@ -44,12 +49,144 @@
 
 def mixer_inputs(normed, first_weight, second_weight):
     empty = jnp.zeros((normed.shape[0], first_weight.shape[1]), jnp.float32)
-    single, double = folders(normed)
+    single, _ = folders(normed)
     result = (
         single(empty, lax.all_gather(first_weight, "fs", axis=0, tiled=True), jnp.int32(0)),
         single(empty, lax.all_gather(second_weight, "fs", axis=0, tiled=True), jnp.int32(0)),
     )
     return result
+
+
+def mover(count, parts, spread, *refs):
+    ins, outs = refs[:count], refs[count : 2 * count]
+    send, recv, pass_send, pass_recv, local = refs[2 * count :]
+    me, rep = lax.axis_index("fs"), lax.axis_index("rep")
+    twin = {"rep": 1 - rep}
+    barrier = pltpu.get_barrier_semaphore()
+    for step in range(1, parts):
+        pl.semaphore_signal(
+            barrier, inc=1, device_id={"fs": lax.rem(me + step, parts)},
+            device_id_type=pl.DeviceIdType.MESH,
+        )
+    pl.semaphore_signal(barrier, inc=1, device_id=twin, device_id_type=pl.DeviceIdType.MESH)
+    pl.semaphore_wait(barrier, parts)
+
+    def block(a, index):
+        return ins[a].at[index] if spread else ins[a].at[0]
+
+    def half(a, which):
+        size = outs[a].shape[1] // 2
+        return pl.ds(pl.multiple_of(which * size, size), size)
+
+    own = [
+        pltpu.make_async_copy(block(a, me), outs[a].at[me], local.at[a]) for a in range(count)
+    ]
+    for copy in own:
+        copy.start()
+
+    def first(step, a):
+        peer = lax.rem(me + step, parts)
+        return pltpu.make_async_remote_copy(
+            src_ref=block(a, peer).at[half(a, rep)],
+            dst_ref=outs[a].at[me, half(a, rep)],
+            send_sem=send.at[a, step],
+            recv_sem=recv.at[a, step],
+            device_id={"fs": peer},
+            device_id_type=pl.DeviceIdType.MESH,
+        )
+
+    def second(step, a):
+        source = lax.rem(me + parts - step, parts)
+        return pltpu.make_async_remote_copy(
+            src_ref=outs[a].at[source, half(a, rep)],
+            dst_ref=outs[a].at[source, half(a, rep)],
+            send_sem=pass_send.at[a, step],
+            recv_sem=pass_recv.at[a, step],
+            device_id=twin,
+            device_id_type=pl.DeviceIdType.MESH,
+        )
+
+    steps = [(step, a) for step in range(1, parts) for a in range(count)]
+    for step, a in steps:
+        first(step, a).start()
+    for step, a in steps:
+        first(step, a).wait_recv()
+        second(step, a).start()
+    for step, a in steps:
+        second(step, a).wait_recv()
+    for step, a in steps:
+        first(step, a).wait_send()
+        second(step, a).wait_send()
+    for copy in own:
+        copy.wait()
+
+
+def moved(arrays, spread, collective_id):
+    parts = lax.axis_size("fs")
+    count = len(arrays)
+    nbytes = sum(2 * x.size for x in arrays) * (1 if spread else parts)
+    pair = pltpu.SemaphoreType.DMA((count, parts))
+    return pl.pallas_call(
+        functools.partial(mover, count, parts, spread),
+        out_shape=[jax.ShapeDtypeStruct((parts,) + x.shape[1:], x.dtype) for x in arrays],
+        in_specs=[pl.BlockSpec(memory_space=pl.ANY)] * count,
+        out_specs=[pl.BlockSpec(memory_space=pl.ANY)] * count,
+        scratch_shapes=[pair, pair, pair, pair, pltpu.SemaphoreType.DMA((count,))],
+        compiler_params=pltpu.CompilerParams(
+            collective_id=collective_id, has_side_effects=True, vmem_limit_bytes=4 * 2**20
+        ),
+        cost_estimate=pl.CostEstimate(flops=0, bytes_accessed=40 * nbytes, transcendentals=0),
+    )(*arrays)
+
+
+def unit_weights(weights, collective_id):
+    gate_weight, up_weight, down_weight = weights
+    parts = lax.axis_size("fs")
+    rows, units = gate_weight.shape
+    cut = [
+        x.reshape(rows, parts, units // parts).transpose(1, 0, 2)
+        for x in (gate_weight, up_weight)
+    ]
+    cut.append(down_weight.reshape(parts, units // parts, rows))
+    gate, up_part, down = moved(cut, True, collective_id)
+    return (
+        gate.reshape(parts * rows, units // parts),
+        up_part.reshape(parts * rows, units // parts),
+        down.transpose(1, 0, 2).reshape(units // parts, parts * rows),
+    )
+
+
+def mixer_weights(first_weight, second_weight, out_weight, collective_id):
+    parts = lax.axis_size("fs")
+    rows, units = first_weight.shape
+    one, two, out = moved(
+        [first_weight[None], second_weight[None], out_weight[None]], False, collective_id
+    )
+    return (
+        one.reshape(parts * rows, units),
+        two.reshape(parts * rows, units),
+        out.transpose(1, 0, 2).reshape(units, parts * rows),
+    )
+
+
+def feed_forward_by_units(stream, gain, weights):
+    rows = lax.all_gather(stream, "fs", axis=0, tiled=True)
+    gate_weight, up_weight, down_weight = weights
+    normed = normalized(rows, gain)
+    hidden = (
+        jax.nn.silu(accumulate(normed, gate_weight)) * accumulate(normed, up_weight)
+    ).astype(jnp.bfloat16)
+    terms = accumulate(hidden, down_weight).astype(jnp.bfloat16)
+    mine = lax.psum_scatter(terms, "tp", scatter_dimension=1, tiled=True)
+    total = lax.psum_scatter(mine, "fs", scatter_dimension=0, tiled=True)
+    return total.astype(jnp.float32), mine
+
+
+def tokens_move(stream, gate_weight):
+    fs = lax.axis_size("fs")
+    rows, units = gate_weight.shape
+    fits = lax.axis_size("rep") == 2 and units % (32 * fs) == 0 and rows % 32 == 0
+    return fits and 2 * stream.size * fs < 3 * gate_weight.size * (fs - 1)
 
 
 def feed_forward(stream, gain, gate_weight, up_weight, down_weight):
@@ -83,12 +220,23 @@
     up_two,
     down_two,
 ):
-    first = (
-        resid.astype(jnp.float32)
-        + 0.5 * feed_forward(resid, norm_gains[0], gate_one, up_one, down_one)
-    ).astype(jnp.bfloat16)
+    by_units = tokens_move(resid, gate_one)
+    if by_units:
+        weights = unit_weights((gate_one, up_one, down_one), 1)
+        total, mine = feed_forward_by_units(resid, norm_gains[0], weights)
+        mine, proj_u, proj_v, proj_out = lax.optimization_barrier(
+            (mine, proj_u, proj_v, proj_out)
+        )
+        proj_u, proj_v, proj_out = mixer_weights(proj_u, proj_v, proj_out, 2)
+    else:
+        total = feed_forward(resid, norm_gains[0], gate_one, up_one, down_one)
+    first = (resid.astype(jnp.float32) + 0.5 * total).astype(jnp.bfloat16)
     mnormed = normalized(first, norm_gains[1])
-    u_part, v_part = mixer_inputs(mnormed, proj_u, proj_v)
+    if by_units:
+        u_part, v_part = accumulate(mnormed, proj_u), accumulate(mnormed, proj_v)
+    else:
+        u_part, v_part = mixer_inputs(mnormed, proj_u, proj_v)
+        proj_out = lax.all_gather(proj_out, "fs", axis=1, tiled=True)
     rows = u_part.shape[0]
     seqs = rows // BLOCK
     local_heads = spatial.shape[0]
@@ -114,17 +262,22 @@
     )
     terms = jnp.dot(
         gated,
-        lax.all_gather(proj_out, "fs", axis=1, tiled=True),
+        proj_out,
         preferred_element_type=jnp.float32,
     )
     branch = lax.psum_scatter(
         terms.astype(jnp.bfloat16), "tp", scatter_dimension=1, tiled=True
     ).astype(jnp.float32)
     second = (first.astype(jnp.float32) + branch).astype(jnp.bfloat16)
-    return (
-        second.astype(jnp.float32)
-        + 0.5 * feed_forward(second, norm_gains[2], gate_two, up_two, down_two)
-    ).astype(jnp.bfloat16)
+    if by_units:
+        second, gate_two, up_two, down_two = lax.optimization_barrier(
+            (second, gate_two, up_two, down_two)
+        )
+        weights = unit_weights((gate_two, up_two, down_two), 3)
+        total, mine = feed_forward_by_units(second, norm_gains[2], weights)
+    else:
+        total = feed_forward(second, norm_gains[2], gate_two, up_two, down_two)
+    return (second.astype(jnp.float32) + 0.5 * total).astype(jnp.bfloat16)
 
 
 def solution(mesh):

time: 1250 us -> 747 us (0.60)
  waiting for transfers between devices: 1160 us -> 415 us
  Pallas kernels: 0 us -> 216 us
  local copies, waits for them, and re-layouts: 0.85 us -> 29.4 us
    all_gather x9 -> x2, waiting for transfers between devices: 1110 us -> 152 us  [feed_forward_by_units(): rows = lax.all_gather(stream, 'fs', axis=0, tiled=True)]
    reduce_scatter x2 -> x4, waiting for transfers between devices: 13.4 us -> 239 us  [the longest x2 186 us: feed_forward_by_units(): total = lax.psum_scatter(mine, 'fs', scatter_dimension=0, tiled=True)]
    pallas_call x0 -> x3, Pallas kernels: none -> 216 us  [moved(): pl.pallas_call(functools.partial(mover, count, parts, spread), out_shape=...]
    dot_general x3 -> x1, matrix products: 34.6 us -> 1.74 us  [body(): terms = jnp.dot(gated, proj_out, preferred_element_type=jnp.float32)]
    all_gather x3, waiting for transfers between devices: 27.2 us -> 0.02 us  [normalized(): whole = lax.all_gather(stream, 'tp', axis=1, tiled=True).astype(jnp.float32)]
    dot_general x4 -> x6, matrix products: 24.2 us -> 49.3 us  [accumulate(): return jnp.dot(left, piece, preferred_element_type=jnp.float32)]
    reduce_scatter x1, waiting for transfers between devices: 6.68 us -> 23.4 us  [body(): lax.psum_scatter(terms.astype(jnp.bfloat16), 'tp', scatter_dimension=1, t...]
    unnamed x22 -> x56, local copies, waits for them, and re-layouts: 0.05 us -> 13.8 us
  transfers between devices with their start and end apart: 15 -> 10, of which waited for: 15 -> 7; matrix products, arithmetic and copies ran while one was open for 3% -> 2% of each run, Pallas kernels for 0% -> 29%
where the time goes in v1:
time: 747 us
  waiting for transfers between devices  415 us (56%)
  Pallas kernels  216 us (29%)
  matrix products  51.4 us (7%)
  local copies, waits for them, and re-layouts  29.4 us (4%)
  other arithmetic  19.9 us (3%)
  between operations  14 us (2%)
    pallas_call x3, Pallas kernels, moved(): pl.pallas_call(functools.partial(mover, count, parts, spread), out_shape=...  216 us
    reduce_scatter x2, waiting for transfers between devices, feed_forward_by_units(): total = lax.psum_scatter(mine, 'fs', scatter_dimension=0, tiled=True)  186 us
    all_gather x2, waiting for transfers between devices, feed_forward_by_units(): rows = lax.all_gather(stream, 'fs', axis=0, tiled=True)  152 us
    reduce_scatter x2, waiting for transfers between devices, feed_forward_by_units(): mine = lax.psum_scatter(terms, 'tp', scatter_dimension=1, tiled=True)  53.2 us
    dot_general x6, matrix products, accumulate(): return jnp.dot(left, piece, preferred_element_type=jnp.float32)  49.3 us
    reduce_scatter x1, waiting for transfers between devices, body(): lax.psum_scatter(terms.astype(jnp.bfloat16), 'tp', scatter_dimension=1, t...  23.4 us
  transfers between devices with their start and end apart: 10, of which 7 were waited for; matrix products, arithmetic and copies ran while one was open for 2% of the time, Pallas kernels for 29%

profile of v1, /device:TPU:0, one launch (start us, length us, event | category | flops | bytes accessed | tf_op | source)
XLA Modules:
  0.0 746.8 jit_solution(7979387633121414589)
XLA Ops:
  7.3 77.7 %all-gather.6.cloned.1.call-done = bf16[2048,1024]{1,0:T(8,128)(2,1)} async-done(((bf16[256,1024]{1,0:T(8,128)(2,1)}), bf16[2048,1024]{1,0:T(8,128)(2,1)}) %all-gather.6.cloned.1.call-update) | async-done | bytes 4194320 | tf_op jit(solution)/shard_map/all_gather | solution.py:173
  86.7 2.5 copy.84
  89.2 1.8 copy.85
  91.1 1.6 copy-done
  92.7 64.9 %shard_map.145 = (bf16[8,256,352]{2,1,0:T(8,128)(2,1)S(1)}, bf16[8,256,352]{2,1,0:T(8,128)(2,1)S(1)}, bf16[8,352,256]{2,1,0:T(8,128)(2,1)S(1)}) custom-call(bf16[8,256,352]{2,1,0:T(8,128)(2,1)S(1)} %bitcast.60, bf16[8,256,352]{2,1,0:T(8,128)(2,1)S(1)} %bitcast.62, bf16[8,352,256]{2,1,0:T(8,128)(2,1)S(1)} %bitcast.67), custom_call_target="tpu_custom_call" | custom-call | bytes 173015040 | tf_op jit(solution)/shard_map/pallas_call | solution.py:129
  159.9 1.3 copy.103
  161.3 5.2 fusion
  166.5 8.4 %fusion.12 = f32[2048,352]{0,1:T(8,128)} fusion(bf16[2048,352]{1,0:T(8,128)(2,1)S(1)} %bitcast.75, bf16[2048,2048]{1,0:T(8,128)(2,1)} %all-gather.8.cloned.1.call-done, f32[2048]{0:T(1024)S(1)} %bitcast.90, f32[2048]{0:T(1024)S(1)} %add_rsqrt_fusion.2), kind=kOutput, calls=%fused_computation.20 | convolution fusion | flops 2969567232 | bytes 12730368 | tf_op jit(solution)/shard_map/dot_general | solution.py:26
  174.9 13.3 %convolution_convert_fusion.1 = bf16[2048,2048]{1,0:T(8,128)(2,1)} fusion(bf16[352,2048]{1,0:T(8,128)(2,1)} %bitcast.83, bf16[2048,352]{1,0:T(8,128)(2,1)S(1)} %bitcast.74, f32[2048,352]{0,1:T(8,128)} %fusion.12, bf16[2048,2048]{1,0:T(8,128)(2,1)} %all-gather.8.cloned.1.call-done, f32[2048]{0:T(1024)S(1)} %bitcast.91, f32[2048]{0:T(1024)S(1)} %add_rsqrt_fusion.2), kind=kOutput, calls=%fused_computation.11 | convolution fusion | flops 5930876928 | bytes 22560768 | tf_op jit(solution)/shard_map/dot_general | solution.py:26
  188.5 26.5 %reduce-scatter.6.cloned.1.call-done = bf16[2048,1024]{1,0:T(8,128)(2,1)} async-done(((bf16[2048,2048]{1,0:T(8,128)(2,1)}), bf16[2048,1024]{1,0:T(8,128)(2,1)}) %reduce-scatter.6.cloned.1.call-update) | async-done | bytes 4194320 | tf_op jit(solution)/shard_map/reduce_scatter | solution.py:180
  215.1 93.0 %reduce-scatter.8.cloned.1.call-done = bf16[256,1024]{1,0:T(8,128)(2,1)} async-done(((bf16[2048,1024]{1,0:T(8,128)(2,1)}), bf16[256,1024]{1,0:T(8,128)(2,1)}) %reduce-scatter.8.cloned.1.call-update) | async-done | bytes 524304 | tf_op jit(solution)/shard_map/reduce_scatter | solution.py:181
  308.2 2.0 add_convert_fusion.2
  310.4 86.5 %shard_map.146 = (bf16[8,256,512]{2,1,0:T(8,128)(2,1)S(1)}, bf16[8,256,512]{2,1,0:T(8,128)(2,1)S(1)}, bf16[8,512,256]{2,1,0:T(8,128)(2,1)S(1)}) custom-call(bf16[1,256,512]{2,1,0:T(8,128)(2,1)S(1)} %bitcast.69, bf16[1,256,512]{2,1,0:T(8,128)(2,1)S(1)} %bitcast.70, bf16[1,512,256]{2,1,0:T(8,128)(2,1)S(1)} %bitcast.71), custom_call_target="tpu_custom_call" | custom-call | bytes 251658240 | tf_op jit(solution)/shard_map/pallas_call | solution.py:129
  398.2 1.4 copy-done.7
  399.6 2.4 copy.96
  402.0 1.5 fusion.14
  403.5 2.9 fusion.31
  406.8 2.9 fusion.38
  413.4 1.7 convolution_convert_fusion.2
  415.2 23.4 %reduce-scatter.10.cloned.1.call-done = bf16[256,1024]{1,0:T(8,128)(2,1)} async-done(((bf16[256,2048]{1,0:T(8,128)(2,1)}), bf16[256,1024]{1,0:T(8,128)(2,1)}) %reduce-scatter.10.cloned.1.call-update) | async-done | bytes 524304 | tf_op jit(solution)/shard_map/reduce_scatter | solution.py:268
  438.6 2.0 add_convert_fusion.1
  440.7 74.1 %all-gather.12.cloned.1.call-done = bf16[2048,1024]{1,0:T(8,128)(2,1)} async-done(((bf16[256,1024]{1,0:T(8,128)(2,1)}), bf16[2048,1024]{1,0:T(8,128)(2,1)}) %all-gather.12.cloned.1.call-update) | async-done | bytes 4194320 | tf_op jit(solution)/shard_map/all_gather | solution.py:173
  516.5 2.5 copy.99
  519.0 1.8 copy.100
  520.9 1.6 copy-done.1
  522.5 64.9 %shard_map.147 = (bf16[8,256,352]{2,1,0:T(8,128)(2,1)S(1)}, bf16[8,256,352]{2,1,0:T(8,128)(2,1)S(1)}, bf16[8,352,256]{2,1,0:T(8,128)(2,1)S(1)}) custom-call(bf16[8,256,352]{2,1,0:T(8,128)(2,1)S(1)} %bitcast.61, bf16[8,256,352]{2,1,0:T(8,128)(2,1)S(1)} %bitcast.63, bf16[8,352,256]{2,1,0:T(8,128)(2,1)S(1)} %bitcast.68), custom_call_target="tpu_custom_call" | custom-call | bytes 173015040 | tf_op jit(solution)/shard_map/pallas_call | solution.py:129
  591.0 5.2 fusion.3
  596.3 8.4 %fusion.9 = f32[2048,352]{0,1:T(8,128)} fusion(bf16[2048,352]{1,0:T(8,128)(2,1)S(1)} %bitcast.77, bf16[2048,2048]{1,0:T(8,128)(2,1)} %all-gather.14.cloned.1.call-done, f32[2048]{0:T(1024)S(1)} %bitcast.86, f32[2048]{0:T(1024)S(1)} %add_rsqrt_fusion.1), kind=kOutput, calls=%fused_computation.19 | convolution fusion | flops 2969567232 | bytes 12730368 | tf_op jit(solution)/shard_map/dot_general | solution.py:26
  604.7 13.3 %convolution_convert_fusion = bf16[2048,2048]{1,0:T(8,128)(2,1)} fusion(bf16[352,2048]{1,0:T(8,128)(2,1)} %bitcast.84, bf16[2048,352]{1,0:T(8,128)(2,1)S(1)} %bitcast.76, f32[2048,352]{0,1:T(8,128)} %fusion.9, bf16[2048,2048]{1,0:T(8,128)(2,1)} %all-gather.14.cloned.1.call-done, f32[2048]{0:T(1024)S(1)} %bitcast.87, f32[2048]{0:T(1024)S(1)} %add_rsqrt_fusion.1), kind=kOutput, calls=%fused_computation.10 | convolution fusion | flops 5930876928 | bytes 22560768 | tf_op jit(solution)/shard_map/dot_general | solution.py:26
  618.1 26.7 %reduce-scatter.12.cloned.1.call-done = bf16[2048,1024]{1,0:T(8,128)(2,1)} async-done(((bf16[2048,2048]{1,0:T(8,128)(2,1)}), bf16[2048,1024]{1,0:T(8,128)(2,1)}) %reduce-scatter.12.cloned.1.call-update) | async-done | bytes 4194320 | tf_op jit(solution)/shard_map/reduce_scatter | solution.py:180
  644.8 93.1 %reduce-scatter.14.cloned.1.call-done = bf16[256,1024]{1,0:T(8,128)(2,1)} async-done(((bf16[2048,1024]{1,0:T(8,128)(2,1)}), bf16[256,1024]{1,0:T(8,128)(2,1)}) %reduce-scatter.14.cloned.1.call-update) | async-done | bytes 524304 | tf_op jit(solution)/shard_map/reduce_scatter | solution.py:181
  737.9 2.0 add_convert_fusion
  (98 shorter events, 16.0 us)
Async XLA Ops:
  6.5 78.5 %copy-start.20 = (bf16[256,2816]{1,0:T(8,128)(2,1)S(1)}, bf16[256,2816]{1,0:T(8,128)(2,1)}, u32[]{:S(2)}) copy-start(bf16[256,2816]{1,0:T(8,128)(2,1)} %param.17) | copy-start | bytes 4325380
  6.5 78.5 %all-gather.6.cloned.1.call-start = ((), (), s32[]{:S(2)}) async-start(), calls=%async_computation.5 | async-start | bytes 4718592 | tf_op jit(solution)/shard_map/all_gather | solution.py:173
  7.3 154.0 %all-gather.8.cloned.1.call-start = ((), (), s32[]{:S(2)}) async-start(), calls=%async_computation.6 | async-start | bytes 12582912 | tf_op jit(solution)/shard_map/all_gather | solution.py:21
  85.0 130.0 %reduce-scatter.6.cloned.1.call-start = ((), (), s32[]{:S(2)}) async-start(), calls=%async_computation.7 | async-start | bytes 12582912 | tf_op jit(solution)/shard_map/reduce_scatter | solution.py:180
  91.1 1.6 copy-start
  92.7 68.5 %copy-start.23 = (f32[3,2048]{1,0:T(4,128)S(1)}, f32[3,2048]{1,0:T(4,128)}, u32[]{:S(2)}) copy-start(f32[3,2048]{1,0:T(4,128)} %param.16) | copy-start | bytes 73732
  161.2 5.2 copy-start.11
  166.5 8.4 %copy-start.9 = (bf16[8,256,352]{2,1,0:T(8,128)(2,1)S(1)}, bf16[8,256,352]{2,1,0:T(8,128)(2,1)}, u32[]{:S(2)}) copy-start(bf16[8,256,352]{2,1,0:T(8,128)(2,1)} %copy-done.8) | copy-start | bytes 4325380
  188.3 119.9 %copy-start.19 = (bf16[256,1024]{1,0:T(8,128)(2,1)S(1)}, bf16[256,1024]{1,0:T(8,128)(2,1)}, u32[]{:S(2)}) copy-start(bf16[256,1024]{1,0:T(8,128)(2,1)} %param.15) | copy-start | bytes 1572868
  188.3 119.8 %reduce-scatter.8.cloned.1.call-start = ((), (), s32[]{:S(2)}) async-start(), calls=%async_computation.8 | async-start | bytes 4718592 | tf_op jit(solution)/shard_map/reduce_scatter | solution.py:181
  215.0 95.3 %copy-start.2 = (bf16[256,512]{1,0:T(8,128)(2,1)S(1)}, bf16[256,512]{1,0:T(8,128)(2,1)}, u32[]{:S(2)}) copy-start(bf16[256,512]{1,0:T(8,128)(2,1)} %param.20) | copy-start | bytes 786436
  215.0 95.3 %copy-start.3 = (bf16[256,512]{1,0:T(8,128)(2,1)S(1)}, bf16[256,512]{1,0:T(8,128)(2,1)}, u32[]{:S(2)}) copy-start(bf16[256,512]{1,0:T(8,128)(2,1)} %param.21) | copy-start | bytes 786436
  215.0 95.3 %copy-start.4 = (bf16[512,256]{1,0:T(8,128)(2,1)S(1)}, bf16[512,256]{1,0:T(8,128)(2,1)}, u32[]{:S(2)}) copy-start(bf16[512,256]{1,0:T(8,128)(2,1)} %param.26) | copy-start | bytes 786436
  215.1 186.9 %all-gather.10.cloned.1.call-start = ((), (), s32[]{:S(2)}) async-start(), calls=%async_computation.9 | async-start | bytes 1572864 | tf_op jit(solution)/shard_map/all_gather | solution.py:21
  310.2 128.4 %reduce-scatter.10.cloned.1.call-start = ((), (), s32[]{:S(2)}) async-start(), calls=%async_computation.10 | async-start | bytes 1572864 | tf_op jit(solution)/shard_map/reduce_scatter | solution.py:268
  398.2 1.4 copy-start.7
  403.5 3.3 copy-start.6
  409.7 2.3 copy-start.24
  409.7 2.9 copy-start.22
  409.7 2.9 copy-start.25
  409.7 3.3 copy-start.26
  411.0 2.4 copy-start.16
  413.0 25.6 %copy-start.17 = (bf16[256,1024]{1,0:T(8,128)(2,1)S(1)}, bf16[256,1024]{1,0:T(8,128)(2,1)}, u32[]{:S(2)}) copy-start(bf16[256,1024]{1,0:T(8,128)(2,1)} %add_convert_fusion.2) | copy-start | bytes 1572868
  415.1 99.8 %copy-start.21 = (bf16[256,2816]{1,0:T(8,128)(2,1)S(1)}, bf16[256,2816]{1,0:T(8,128)(2,1)}, u32[]{:S(2)}) copy-start(bf16[256,2816]{1,0:T(8,128)(2,1)} %param.27) | copy-start | bytes 4325380
  415.1 99.7 %all-gather.12.cloned.1.call-start = ((), (), s32[]{:S(2)}) async-start(), calls=%async_computation.11 | async-start | bytes 4718592 | tf_op jit(solution)/shard_map/all_gather | solution.py:173
  440.7 150.3 %all-gather.14.cloned.1.call-start = ((), (), s32[]{:S(2)}) async-start(), calls=%async_computation.12 | async-start | bytes 12582912 | tf_op jit(solution)/shard_map/all_gather | solution.py:21
  514.9 130.0 %reduce-scatter.12.cloned.1.call-start = ((), (), s32[]{:S(2)}) async-start(), calls=%async_computation.13 | async-start | bytes 12582912 | tf_op jit(solution)/shard_map/reduce_scatter | solution.py:180
  520.9 1.6 copy-start.1
  591.0 5.2 copy-start.15
  596.3 8.4 %copy-start.13 = (bf16[8,256,352]{2,1,0:T(8,128)(2,1)S(1)}, bf16[8,256,352]{2,1,0:T(8,128)(2,1)}, u32[]{:S(2)}) copy-start(bf16[8,256,352]{2,1,0:T(8,128)(2,1)} %copy-done.12) | copy-start | bytes 4325380
  618.1 119.9 %copy-start.18 = (bf16[256,1024]{1,0:T(8,128)(2,1)S(1)}, bf16[256,1024]{1,0:T(8,128)(2,1)}, u32[]{:S(2)}) copy-start(bf16[256,1024]{1,0:T(8,128)(2,1)} %add_convert_fusion.1) | copy-start | bytes 1572868
  618.1 119.8 %reduce-scatter.14.cloned.1.call-start = ((), (), s32[]{:S(2)}) async-start(), calls=%async_computation.14 | async-start | bytes 4718592 | tf_op jit(solution)/shard_map/reduce_scatter | solution.py:181
  (5 other events, 6.0 us)
Sparse Core Ops, SparseCore 0:
  9.5 75.5 all-gather.5
  86.5 18.3 all-gather.7
  188.4 26.5 reduce-scatter.5
  218.5 89.5 reduce-scatter.7
  310.3 8.6 all-gather.9
  415.3 23.3 reduce-scatter.9
  440.8 73.9 all-gather.11
  516.4 18.3 all-gather.13
  618.2 26.5 reduce-scatter.11
  648.3 89.5 reduce-scatter.13
